TPU v7x, 32 devices: a whole 2x2x4 slice. The times are simulated.
32 devices in a mesh: sp: 16 (over z, y, x), tp: 2 (over core).
Axes of the slice: x: 2, y: 2, z: 4, core: 2. Of those that a mesh axis runs over, the one named last changes fastest.
Arguments:
- conv_value: bfloat16 [8192, 1536], P('sp', 'tp'), may hold values from -6 to 6
- conv_gate: bfloat16 [8192, 1536], P('sp', 'tp'), may hold values from -8 to 8
- conv_out: bfloat16 [8192, 1536], P('sp', 'tp'), may hold values from -40 to 40
- conv_taps: bfloat16 [31, 1536], P(None, 'tp'), may hold values from -1 to 1
- norm_gain: float32 [1536], P('tp'), may hold values from 0.1 to 1.9
- norm_shift: float32 [1536], P('tp'), may hold values from -3 to 3
- proj_weight: bfloat16 [2048, 1536], P(None, 'tp'), may hold values from -0.15625 to 0.15625
- out_grad: bfloat16 [8192, 2048], P('sp'), may hold values from -6 to 6
Outputs:
- grad_value: bfloat16 [8192, 1536], P('sp', 'tp')
- grad_gate: bfloat16 [8192, 1536], P('sp', 'tp')
- grad_taps: float32 [31, 1536], P(None, 'tp')
- grad_gain: float32 [1536], P('tp')
- grad_shift: float32 [1536], P('tp')
- grad_proj: float32 [2048, 1536], P('sp', 'tp')
All inputs are finite; a program needn't handle non-finite values.
Results may differ from a plain program's by a relative error of at most 0.005.
Values may be sent and summed in bfloat16 or wider, within the bound.
A program may use at most 64 MiB of HBM per device.

v0:
```python
import jax
import jax.numpy as jnp
from jax import lax
from jax.sharding import PartitionSpec as P

norm_eps = 1e-05


def padded(array, sides, width):
    for axis, dim in sides:
        peers, length = (lax.axis_size(axis), array.shape[dim])
        up = [(i, (i + 1) % peers) for i in range(peers - 1)]
        down = [(j, i) for i, j in up]
        last = lax.slice_in_dim(array, length - width, length, axis=dim)
        first = lax.slice_in_dim(array, 0, width, axis=dim)
        before = lax.ppermute(last, axis, up)
        after = lax.ppermute(first, axis, down)
        array = jnp.concatenate([before, array, after], axis=dim)
    return array


def project_rows(out_grad, active):
    return lax.psum_scatter(
        lax.dot_general(
            out_grad, active, (((0,), (0,)), ((), ())), preferred_element_type=jnp.float32
        ),
        "sp",
        scatter_dimension=0,
        tiled=True,
    )


def local(conv_value, conv_gate, conv_out, conv_taps, norm_gain, norm_shift, proj_weight, out_grad):
    seq_rows, chan_local = conv_value.shape
    tap_reach = conv_taps.shape[0] - 1
    chan_total = chan_local * lax.axis_size("tp")
    height = conv_out.astype(jnp.float32)
    center = lax.psum(jnp.sum(height, axis=1), "tp") / chan_total
    centered = height - center[:, None]
    variance = lax.psum(jnp.sum(centered * centered, axis=1), "tp") / chan_total
    inv_std = lax.rsqrt(variance + norm_eps)[:, None]
    normed = centered * inv_std
    shifted = normed * norm_gain + norm_shift
    sig_norm = jax.nn.sigmoid(shifted)
    active = (shifted * sig_norm).astype(jnp.bfloat16)
    act_grad = jnp.dot(out_grad, proj_weight, preferred_element_type=jnp.float32)
    norm_grad = act_grad * (sig_norm * (1.0 + shifted * (1.0 - sig_norm)))
    scaled = norm_grad * norm_gain
    grad_sum, grad_dot = lax.psum((jnp.sum(scaled, axis=1), jnp.sum(scaled * normed, axis=1)), "tp")
    height_grad = inv_std * (
        scaled - grad_sum[:, None] / chan_total - normed * (grad_dot[:, None] / chan_total)
    )
    sig_gate = jax.nn.sigmoid(conv_gate.astype(jnp.float32))
    value_float = conv_value.astype(jnp.float32)
    gated_rows = (value_float * sig_gate).astype(jnp.bfloat16)
    tap_values = conv_taps.astype(jnp.float32)
    edge_rows = jnp.concatenate(
        [height_grad[:tap_reach], gated_rows[seq_rows - tap_reach :].astype(jnp.float32)], axis=0
    )
    framed = padded(edge_rows, (("sp", 0),), tap_reach)
    earlier = framed[:tap_reach]
    later = framed[3 * tap_reach :]
    extended = jnp.concatenate([earlier, gated_rows.astype(jnp.float32)], axis=0)
    ahead_grad = jnp.concatenate([height_grad, later], axis=0)
    gated_grad = jnp.zeros((seq_rows, chan_local), jnp.float32)
    for tap_index in range(tap_reach + 1):
        begin = tap_reach - tap_index
        gated_grad = gated_grad + tap_values[tap_index] * ahead_grad[begin : begin + seq_rows]
    tap_rows = jnp.stack(
        [
            jnp.sum(height_grad * extended[tap_index : tap_index + seq_rows], axis=0)
            for tap_index in range(tap_reach + 1)
        ]
    )
    gain_row = jnp.sum(norm_grad * normed, axis=0)
    shift_row = jnp.sum(norm_grad, axis=0)
    grad_taps, grad_gain, grad_shift = lax.psum((tap_rows, gain_row, shift_row), "sp")
    grad_value = (gated_grad * sig_gate).astype(jnp.bfloat16)
    grad_gate = (gated_grad * value_float * sig_gate * (1.0 - sig_gate)).astype(jnp.bfloat16)
    grad_proj = project_rows(out_grad, active)
    return (grad_value, grad_gate, grad_taps, grad_gain, grad_shift, grad_proj)


def solution(mesh):
    in_specs = (
        P("sp", "tp"),
        P("sp", "tp"),
        P("sp", "tp"),
        P(None, "tp"),
        P("tp"),
        P("tp"),
        P(None, "tp"),
        P("sp", None),
    )
    out_specs = (P("sp", "tp"), P("sp", "tp"), P(None, "tp"), P("tp"), P("tp"), P("sp", "tp"))
    return jax.shard_map(local, mesh=mesh, in_specs=in_specs, out_specs=out_specs, check_vma=False)
```

profile of v0, /device:TPU:0, one launch (start us, length us, event | category | flops | bytes accessed | tf_op | source)
XLA Modules:
  0.0 290.8 jit_solution(6177124054448925998)
XLA Ops:
  7.2 1.5 convert_reduce_fusion
  8.7 2.6 psum.49
  11.3 1.5 fusion.21
  12.8 2.5 psum.50
  15.3 6.6 %convolution_bitcast_fusion = f32[2048,768]{0,1:T(8,128)} fusion(bf16[512,2048]{1,0:T(8,128)(2,1)} %param.15, bf16[512,768]{1,0:T(8,128)(2,1)} %param.10, f32[768]{0:T(1024)S(1)} %copy-done.11, f32[768]{0:T(1024)S(1)} %copy-done.9, f32[512]{0:T(512)S(1)} %add_rsqrt_fusion, f32[512]{0:T(512)S(1)} %broadcast_multiply_fusion.2), kind=kOutput, calls=%fused_computation.58 | convolution fusion | flops 1614544896 | bytes 9185280 | tf_op jit(solution)/shard_map/dot_general | solution.py:24
  22.0 3.2 %fusion.212 = (f32[512,768]{1,0:T(8,128)}, bf16[512,768]{1,0:T(8,128)(2,1)S(1)}) fusion(bf16[512,768]{1,0:T(8,128)(2,1)} %param.9, bf16[512,768]{1,0:T(8,128)(2,1)} %param.8), kind=kLoop, calls=%fused_computation.332 | loop fusion | flops 3145728 | bytes 3932160 | tf_op jit(solution)/shard_map/convert_element_type | solution.py:63
  25.2 0.9 copy-done.5
  26.1 4.7 %collective-permute-start.1 = (f32[30,768]{1,0:T(8,128)S(1)}, f32[30,768]{1,0:T(8,128)S(1)}, u32[]{:S(2)}, u32[]{:S(2)}) collective-permute-start(f32[30,768]{1,0:T(8,128)S(1)} %slice_convert_fusion), channel_id=1, source_target_pairs={{0,2},{2,4},{4,6},{6,8},{8,10},{10,12},{12,14},{14,16},{16,18},{18... | collective-permute-start | bytes 276488 | tf_op jit(solution)/shard_map/ppermute | solution.py:16
  30.9 3.7 %fusion.20 = (f32[768]{0:T(1024)S(1)}, f32[512]{0:T(512)S(1)}, f32[512]{0:T(512)S(1)}, f32[768]{0:T(1024)S(1)}, f32[512,768]{1,0:T(8,128)}) fusion(bf16[512,768]{1,0:T(8,128)(2,1)S(1)} %copy-done.3, f32[512]{0:T(512)S(1)} %add_rsqrt_fusion, f32[512]{0:T(512)S(1)} %broadcast_multiply_fusion.2, f32[768]{0:T(1024)S(1)} %copy-done.9, f32[768]{0:T(1024)S(1)} %copy-done.11, ...), kind=kOutput, calls=%fused_computation.83 | convolution fusion | flops 1618474496 | bytes 7622656 | tf_op jit(solution)/shard_map/dot_general | solution.py:46
  34.5 2.4 all-reduce.1
  37.0 41.7 %all-reduce = (f32[768]{0:T(1024)}, f32[768]{0:T(1024)}) all-reduce(f32[768]{0:T(1024)S(1)} %get-tuple-element.42, f32[768]{0:T(1024)S(1)} %get-tuple-element.45), channel_id=1, replica_groups=mesh['sp'=16,'tp'=2] {'sp'}, use_global_device_ids=true, to_apply=%region_41.0 | all-reduce | flops 1536 | bytes 12288 | tf_op jit(solution)/shard_map/psum | solution.py:77
  78.7 0.2 slice_reduce_fusion.30
  78.9 0.7 slice_reduce_fusion.29
  79.6 12.5 %fusion.202 = (f32[768]{0:T(1024)S(1)}, f32[768]{0:T(1024)S(1)}, f32[768]{0:T(1024)S(1)}, f32[768]{0:T(1024)S(1)}, f32[768]{0:T(1024)S(1)}, /*index=5*/f32[768]{...) fusion(f32[512,768]{1,0:T(8,128)} %get-tuple-element.83, ...), kind=kLoop, calls=%fused_computation.266 | loop fusion | flops 13755648 | bytes 5636096 | tf_op jit(solution)/shard_map/reduce_sum | solution.py:71
  92.1 1.5 collective-permute-start
  93.6 2.4 fusion.64
  96.1 2.3 fusion.91
  98.4 0.8 fusion.37
  99.5 0.6 stack.114
  100.1 0.6 stack.113
  100.7 0.6 stack.112
  101.3 0.6 stack.111
  101.9 0.6 stack.110
  102.5 0.6 stack.109
  103.0 0.6 stack.108
  103.6 4.0 %stack.127 = f32[31,768]{1,0:T(8,128)} concatenate(f32[1,768]{1,0:T(1,128)S(1)} %stack.96, f32[1,768]{1,0:T(1,128)S(1)} %stack.97, f32[1,768]{1,0:T(1,128)S(1)} %stack.98, f32[1,768]{1,0:T(1,128)S(1)} %stack.99, f32[1,768]{1,0:T(1,128)S(1)} %stack.100, f32[1,768]{1,0:T(1,128)S(1)} %stack.101, f32[1,768]{1,0:T(1,128)S(1)} %stack.102, f32[1,768]{1,0:T(1,128)S(1)} %stack.103, ...), dimensions={0} | concatenate | bytes 190464 | tf_op jit(solution)/shard_map/stack | solution.py:69
  107.7 30.6 %fusion.24 = (bf16[512,768]{1,0:T(8,128)(2,1)}, f32[512,768]{1,0:T(8,128)}) fusion(bf16[512,768]{1,0:T(8,128)(2,1)} %param.8, bf16[512,768]{1,0:T(8,128)(2,1)} %param.9, f32[512,768]{1,0:T(8,128)} %copy-done.1, f32[768]{0:T(1024)S(1)} %get-tuple-element.48, f32[30,768]{1,0:T(8,128)S(1)} %collective-permute-done, f32[768]{0:T(1024)S(1)} %get-tuple-element.49, ...), kind=kLoop, calls=%fused_computation.87 | loop fusion | flops 39714816 | bytes 5692416 | tf_op jit(solution)/shard_map/convert_element_type | solution.py:79
  138.3 2.7 multiply_convert_fusion
  141.0 32.0 %reduce-scatter.2.cloned.1.call-done = f32[128,768]{0,1:T(8,128)} async-done(((f32[2048,768]{0,1:T(8,128)}), f32[128,768]{0,1:T(8,128)}) %reduce-scatter.2.cloned.1.call-update) | async-done | bytes 393232 | tf_op jit(solution)/shard_map/reduce_scatter | solution.py:23
  173.0 1.9 copy.14
  174.9 107.5 %all-reduce.4.cloned.1.call-done = f32[31,768]{1,0:T(8,128)} async-done(((f32[31,768]{1,0:T(8,128)}), f32[31,768]{1,0:T(8,128)}) %all-reduce.4.cloned.1.call-update) | async-done | bytes 95248 | tf_op jit(solution)/shard_map/psum | solution.py:77
  282.4 1.5 copy.16
  (59 shorter events, 0.3 us)
Async XLA Ops:
  7.2 23.7 %copy-start = (bf16[2048,768]{1,0:T(8,128)(2,1)S(1)}, bf16[2048,768]{1,0:T(8,128)(2,1)}, u32[]{:S(2)}) copy-start(bf16[2048,768]{1,0:T(8,128)(2,1)} %param.14) | copy-start | bytes 9437188
  7.2 8.1 %copy-start.9 = (f32[768]{0:T(1024)S(1)}, f32[768]{0:T(1024)}, u32[]{:S(2)}) copy-start(f32[768]{0:T(1024)} %param.12) | copy-start | bytes 9220
  7.2 8.1 %copy-start.11 = (f32[768]{0:T(1024)S(1)}, f32[768]{0:T(1024)}, u32[]{:S(2)}) copy-start(f32[768]{0:T(1024)} %param.13) | copy-start | bytes 9220
  7.2 165.8 %reduce-scatter.2.cloned.1.call-start = ((), (), s32[]{:S(2)}) async-start(), calls=%async_computation.2 | async-start | bytes 6684672 | tf_op jit(solution)/shard_map/reduce_scatter | solution.py:23
  15.3 15.5 %copy-start.8 = (f32[512]{0:T(512)}, f32[512]{0:T(512)S(1)}, u32[]{:S(2)}) copy-start(f32[512]{0:T(512)S(1)} %add_rsqrt_fusion) | copy-start | bytes 6148
  21.9 8.9 %copy-start.7 = (bf16[31,768]{1,0:T(8,128)(2,1)S(1)}, bf16[31,768]{1,0:T(8,128)(2,1)}, u32[]{:S(2)}) copy-start(bf16[31,768]{1,0:T(8,128)(2,1)} %param.11) | copy-start | bytes 142852
  21.9 260.5 %all-reduce.4.cloned.1.call-start = ((), (), s32[]{:S(2)}) async-start(), calls=%async_computation.1 | async-start | bytes 196608 | tf_op jit(solution)/shard_map/psum | solution.py:77
  22.0 8.9 %copy-start.3 = (bf16[512,768]{1,0:T(8,128)(2,1)S(1)}, bf16[512,768]{1,0:T(8,128)(2,1)}, u32[]{:S(2)}) copy-start(bf16[512,768]{1,0:T(8,128)(2,1)} %param.10) | copy-start | bytes 2359300
  22.0 8.9 %copy-start.10 = (bf16[512,2048]{1,0:T(8,128)(2,1)S(1)}, bf16[512,2048]{1,0:T(8,128)(2,1)}, u32[]{:S(2)}) copy-start(bf16[512,2048]{1,0:T(8,128)(2,1)} %param.15) | copy-start | bytes 6291460
  25.2 0.9 copy-start.5
  26.1 53.5 %collective-permute-start.1 = (f32[30,768]{1,0:T(8,128)S(1)}, f32[30,768]{1,0:T(8,128)S(1)}, u32[]{:S(2)}, u32[]{:S(2)}) collective-permute-start(f32[30,768]{1,0:T(8,128)S(1)} %slice_convert_fusion), channel_id=1, source_target_pairs={{0,2},{2,4},{4,6},{6,8},{8,10},{10,12},{12,14},{14,16},{16,18},{18... | collective-permute-start | bytes 276488 | tf_op jit(solution)/shard_map/ppermute | solution.py:16
  79.6 14.0 %copy-start.2 = (f32[512,768]{1,0:T(8,128)S(1)}, f32[512,768]{1,0:T(8,128)}, u32[]{:S(2)}) copy-start(f32[512,768]{1,0:T(8,128)} %get-tuple-element.83) | copy-start | bytes 4718596
  92.1 6.3 %copy-start.1 = (f32[512,768]{1,0:T(8,128)}, f32[512,768]{1,0:T(8,128)S(1)}, u32[]{:S(2)}) copy-start(f32[512,768]{1,0:T(8,128)S(1)} %get-tuple-element.82) | copy-start | bytes 4718596
  92.1 15.5 %collective-permute-start = (f32[30,768]{1,0:T(8,128)S(1)}, f32[30,768]{1,0:T(8,128)S(1)}, u32[]{:S(2)}, u32[]{:S(2)}) collective-permute-start(f32[30,768]{1,0:T(8,128)S(1)} %slice.373), channel_id=1, source_target_pairs={{2,0},{4,2},{6,4},{8,6},{10,8},{12,10},{14,12},{16,14},{18,16},{20... | collective-permute-start | bytes 276488 | tf_op jit(solution)/shard_map/ppermute | solution.py:17
  96.0 2.4 copy-start.6
  107.7 30.6 %copy-start.4 = (bf16[512,768]{1,0:T(8,128)(2,1)S(1)}, bf16[512,768]{1,0:T(8,128)(2,1)}, u32[]{:S(2)}) copy-start(bf16[512,768]{1,0:T(8,128)(2,1)} %param.9) | copy-start | bytes 2359300
Sparse Core Ops, SparseCore 0:
  22.1 150.8 reduce-scatter.1
  179.0 103.3 all-reduce.3
where the time goes:
time: 291 us
  waiting for transfers between devices  140 us (48%)
  other arithmetic  57.5 us (20%)
  blocking collectives  49.3 us (17%)
  between operations  14.5 us (5%)
  local copies, waits for them, and re-layouts  13.4 us (5%)
  matrix products  10.2 us (4%)
  starting transfers between devices  6.26 us (2%)
    psum x1, waiting for transfers between devices, local(): lax.psum((tap_rows, gain_row, shift_row), 'sp')  108 us
    psum x1, blocking collectives, local(): lax.psum((tap_rows, gain_row, shift_row), 'sp')  41.7 us
    reduce_scatter x1, waiting for transfers between devices, project_rows(): lax.psum_scatter(lax.dot_general(out_grad, active, (((0,), (0,)), ((), ()...  32 us
    convert_element_type x1, other arithmetic, local(): (gated_grad * value_float * sig_gate * (1.0 - sig_gate)).astype(jnp.bfloa...  30.6 us
    reduce_sum x4, other arithmetic, local(): jnp.sum(height_grad * extended[tap_index:tap_index + seq_rows], axis=0)  18.1 us
    another operation x32, local copies, waits for them, and re-layouts, local(): jnp.stack([jnp.sum(height_grad * extended[tap_index:tap_index + seq_rows]...  8.2 us
    dot_general x1, matrix products, project_rows(): lax.dot_general(out_grad, active, (((0,), (0,)), ((), ())), preferred_ele...  6.56 us
  transfers between devices with their start and end apart: 4, of which 2 were waited for; matrix products, arithmetic and copies ran while one was open for 24% of the time, Pallas kernels for 0%

commit v1 on v0

v1 whole, which is shorter than its diff:
```python
import functools

import jax
import jax.numpy as jnp
from jax import lax
from jax.experimental import pallas as pl
from jax.experimental.pallas import tpu as pltpu
from jax.sharding import PartitionSpec as P

norm_eps = 1e-05
MESH = pl.DeviceIdType.MESH
F32 = jnp.float32
BF16 = jnp.bfloat16
LANES = 128


def bit(x, b):
    return lax.rem(x // (1 << b), 2)


def coordinate_bits(index, nbits):
    bits = [bit(index, b) for b in range(nbits)]
    if nbits >= 2:
        bits[nbits - 2] = lax.rem(bits[nbits - 2] + bits[nbits - 1], 2)
    return bits


def partner_of(me, b, nbits):
    def flip(x, c):
        return x + (1 << c) * (1 - 2 * bit(me, c))

    other = flip(me, b)
    if nbits >= 2 and b == nbits - 1:
        other = flip(other, b - 1)
    return other


def stage_orders(nbits, groups):
    body = list(range(max(nbits - 1, 1)))
    tail = list(range(len(body), nbits))
    return [body[g % len(body):] + body[: g % len(body)] + tail for g in range(groups)]


def kernel(
    dims,
    cv_hbm, cg_hbm, co_hbm, taps_ref, gain_ref, shift_ref, w_hbm, og_hbm,
    gv_hbm, gg_hbm, small_out, proj_out,
    cv, cg, co, w, og, ogt, active, normed, dsilu, scaled, hgx, gv, gg,
    st_a, st_b, st_c, st_d, acc, sendbuf, recvbuf, tapacc, rowacc, flat, parts, mine, whole,
    in_sem, out_sem, tp_send, tp_recv, halo_send, halo_recv,
    rs_send, rs_recv, a_send, a_recv, b_send, b_recv,
):
    n, nbits, groups, chan_total = dims
    rows, chan = co.shape
    width = og.shape[1]
    block = width // n
    gcols = chan // groups
    cblocks = chan // LANES
    ntaps = taps_ref.shape[1]
    reach = ntaps - 1
    halo = hgx.shape[1] - rows
    chunk = mine.shape[0]
    per = small_out.shape[0]
    me = lax.axis_index("sp")
    core = lax.axis_index("tp")
    other_core = 1 - core
    orders = stage_orders(nbits, groups)

    loads = [
        pltpu.make_async_copy(src, dst, in_sem.at[i])
        for i, (src, dst) in enumerate(
            ((co_hbm, co), (og_hbm, og), (w_hbm, w), (cg_hbm, cg), (cv_hbm, cv))
        )
    ]
    for copy in loads:
        copy.start()

    barrier = pltpu.get_barrier_semaphore()

    def greet(i, carry):
        pl.semaphore_signal(
            barrier, inc=1, device_id=(lax.rem(me + i, n), core), device_id_type=MESH
        )
        return carry

    lax.fori_loop(1, n, greet, 0)
    pl.semaphore_signal(barrier, inc=1, device_id=(me, other_core), device_id_type=MESH)

    lane_low = lax.broadcasted_iota(jnp.int32, (1, LANES), 1) < LANES // 2

    loads[0].wait()

    def stats(i, carry):
        at = pl.ds(pl.multiple_of(i * 64, 64), 64)
        h = co[at, :].astype(F32)
        mean = jnp.sum(h, axis=1, keepdims=True) / chan
        d = h - mean
        m2 = jnp.sum(d * d, axis=1, keepdims=True)
        st_a[at, :] = jnp.where(lane_low, mean, m2)
        return carry

    lax.fori_loop(0, rows // 64, stats, 0)
    pl.semaphore_wait(barrier, n)
    swap_a = pltpu.make_async_remote_copy(
        src_ref=st_a, dst_ref=st_b, send_sem=tp_send.at[0], recv_sem=tp_recv.at[0],
        device_id=(me, other_core), device_id_type=MESH,
    )
    swap_a.start()

    loads[1].wait()
    mybits = coordinate_bits(me, nbits)
    sub = LANES // block

    def transpose(c, carry):
        t = og[:, pl.ds(pl.multiple_of(c * LANES, LANES), LANES)].T
        for s in range(sub):
            rbits = coordinate_bits(c * sub + s, nbits)
            piece = t[s * block:(s + 1) * block, :]
            for g in range(groups):
                place = 0
                for k, b in enumerate(orders[g]):
                    place = place + lax.rem(rbits[b] + mybits[b], 2) * (1 << (nbits - 1 - k))
                ogt[g, place] = piece
        return carry

    lax.fori_loop(0, width // LANES, transpose, 0)

    swap_a.wait()
    half = 0.5 * chan

    def norm(i, carry):
        at = pl.ds(pl.multiple_of(i * 32, 32), 32)
        own, peer = st_a[at, :], st_b[at, :]
        mean_a, mean_b = own[:, :1], peer[:, :1]
        m2 = own[:, LANES // 2:LANES // 2 + 1] + peer[:, LANES // 2:LANES // 2 + 1]
        gap = mean_a - mean_b
        center = 0.5 * (mean_a + mean_b)
        inv = lax.rsqrt((m2 + gap * gap * half) / chan_total + norm_eps)
        z = (co[at, :].astype(F32) - center) * inv
        normed[at, :] = z
        x = z * gain_ref[...] + shift_ref[...]
        sig = jax.nn.sigmoid(x)
        active[at, :] = (x * sig).astype(BF16)
        dsilu[at, :] = sig * (1.0 + x * (1.0 - sig))
        st_d[at, :] = jnp.broadcast_to(inv, (32, LANES))
        return carry

    lax.fori_loop(0, rows // 32, norm, 0)

    def stage_copy(g, k):
        count = n >> (k + 1)
        off = n - (n >> k)
        return pltpu.make_async_remote_copy(
            src_ref=sendbuf.at[g, pl.ds(off, count)],
            dst_ref=recvbuf.at[g, pl.ds(off, count)],
            send_sem=rs_send.at[g, k],
            recv_sem=rs_recv.at[g, k],
            device_id=(partner_of(me, orders[g][k], nbits), core),
            device_id_type=MESH,
        )

    unit = max(1, n // 4)

    def product(g, start):
        lhs = ogt[g, pl.ds(start, unit)].reshape(unit * block, rows)
        out = jnp.dot(lhs, active[:, g * gcols:(g + 1) * gcols], preferred_element_type=F32)
        return out.reshape(unit, block, gcols)

    for g in range(groups):

        def far(i, carry, g=g):
            sendbuf[g, pl.ds(i * unit, unit)] = product(g, n // 2 + i * unit).astype(BF16)
            return carry

        lax.fori_loop(0, n // 2 // unit, far, 0)
        stage_copy(g, 0).start()
    for g in range(groups):

        def near(i, carry, g=g):
            acc[g, pl.ds(i * unit, unit)] = product(g, i * unit)
            return carry

        lax.fori_loop(0, n // 2 // unit, near, 0)

    def stage(k):
        count = n >> (k + 1)
        off = n - (n >> k)
        for g in range(groups):
            stage_copy(g, k).wait_recv()
            if k + 1 < nbits:
                keep = count // 2

                def pass_on(i, carry, g=g):
                    sendbuf[g, off + count + i] = (
                        acc[g, keep + i] + recvbuf[g, off + keep + i].astype(F32)
                    ).astype(BF16)
                    return carry

                lax.fori_loop(0, count - keep, pass_on, 0)
                stage_copy(g, k + 1).start()
            else:
                keep = count

            def take(i, carry, g=g):
                acc[g, i] = acc[g, i] + recvbuf[g, off + i].astype(F32)
                return carry

            lax.fori_loop(0, keep, take, 0)

    loads[2].wait()
    rowacc[...] = jnp.zeros_like(rowacc)

    def act(i, carry):
        at = pl.ds(pl.multiple_of(i * 128, 128), 128)
        scaled[at, :] = jnp.dot(og[at, :], w[...], preferred_element_type=F32)
        return carry

    lax.fori_loop(0, rows // 128, act, 0)

    def grads(i, carry):
        at = pl.ds(pl.multiple_of(i * 32, 32), 32)
        z = normed[at, :]
        ng = scaled[at, :] * dsilu[at, :]
        ngz = ng * z
        rowacc[0] = rowacc[0] + jnp.sum(ngz.reshape(4, 8, chan), axis=0)
        rowacc[1] = rowacc[1] + jnp.sum(ng.reshape(4, 8, chan), axis=0)
        gain = gain_ref[...]
        s = ng * gain
        scaled[at, :] = s
        total = jnp.sum(s, axis=1, keepdims=True)
        dot = jnp.sum(s * z, axis=1, keepdims=True)
        st_a[at, :] = jnp.where(lane_low, total, dot)
        return carry

    lax.fori_loop(0, rows // 32, grads, 0)
    swap_b = pltpu.make_async_remote_copy(
        src_ref=st_a, dst_ref=st_c, send_sem=tp_send.at[1], recv_sem=tp_recv.at[1],
        device_id=(me, other_core), device_id_type=MESH,
    )
    swap_b.start()
    tapacc[...] = jnp.zeros_like(tapacc)
    flat[...] = jnp.zeros_like(flat)
    swap_b.wait()

    def height(i, carry):
        at = pl.ds(pl.multiple_of(i * 32, 32), 32)
        sums = (st_a[at, :] + st_c[at, :]) / chan_total
        inv = st_d[at, :]
        total, dot = sums[:, :1], sums[:, LANES // 2:LANES // 2 + 1]
        hg = inv[:, :1] * (scaled[at, :] - total - normed[at, :] * dot)
        for c in range(cblocks):
            hgx[c, at, :] = hg[:, c * LANES:(c + 1) * LANES]
        return carry

    height(0, 0)
    halo_copy = pltpu.make_async_remote_copy(
        src_ref=hgx.at[:, pl.ds(0, halo)],
        dst_ref=hgx.at[:, pl.ds(rows, halo)],
        send_sem=halo_send, recv_sem=halo_recv,
        device_id=(lax.rem(me + n - 1, n), core), device_id_type=MESH,
    )

    @pl.when(me > 0)
    def _():
        halo_copy.start()

    lax.fori_loop(1, rows // 32, height, 0)

    @pl.when(me == n - 1)
    def _():
        hgx[:, rows:, :] = jnp.zeros((cblocks, halo, LANES), F32)

    loads[3].wait()
    loads[4].wait()
    stage(0)

    @pl.when(me < n - 1)
    def _():
        halo_copy.wait_recv()

    step = 64
    steps = rows // step

    def conv(i, carry):
        c = i // steps
        r = pl.multiple_of(lax.rem(i, steps) * step, step)
        at = pl.ds(r, step)
        cols = pl.ds(pl.multiple_of(c * LANES, LANES), LANES)
        sig = jax.nn.sigmoid(cg[at, cols].astype(F32))
        value = cv[at, cols].astype(F32)
        gated = (value * sig).astype(BF16).astype(F32)
        total = jnp.zeros((step, LANES), F32)
        for j in range(ntaps):
            h = hgx[c, pl.ds(r + reach - j, step), :]
            total = total + taps_ref[c, pl.ds(j, 1), :] * h
            tapacc[c, j] = tapacc[c, j] + jnp.sum((gated * h).reshape(step // 8, 8, LANES), axis=0)
        gv[at, cols] = (total * sig).astype(BF16)
        gg[at, cols] = (total * value * sig * (1.0 - sig)).astype(BF16)
        return carry

    cuts = [cblocks * steps * i // nbits for i in range(nbits + 1)]
    for k in range(nbits - 1):
        lax.fori_loop(cuts[k], cuts[k + 1], conv, 0)
        if k + 1 < nbits - 1:
            stage(k + 1)
    lax.fori_loop(cuts[nbits - 1], cuts[nbits], conv, 0)

    stores = [
        pltpu.make_async_copy(src, dst, out_sem.at[i])
        for i, (src, dst) in enumerate(((gv, gv_hbm), (gg, gg_hbm)))
    ]
    for copy in stores:
        copy.start()

    for c in range(cblocks):
        rowsum = jnp.sum(tapacc[c], axis=1)
        flat[c * per:c * per + ntaps, :] = rowsum
        for j in range(2):
            flat[c * per + ntaps + j:c * per + ntaps + j + 1, :] = jnp.sum(
                rowacc[j, :, c * LANES:(c + 1) * LANES], axis=0, keepdims=True
            )

    def spread(i):
        peer = lax.rem(me + i, n)
        return pltpu.make_async_remote_copy(
            src_ref=flat.at[pl.ds(pl.multiple_of(peer * chunk, chunk), chunk)],
            dst_ref=parts.at[me],
            send_sem=a_send.at[peer], recv_sem=a_recv.at[me],
            device_id=(peer, core), device_id_type=MESH,
        )

    def collect(i):
        peer = lax.rem(me + i, n)
        return pltpu.make_async_remote_copy(
            src_ref=mine,
            dst_ref=whole.at[pl.ds(pl.multiple_of(me * chunk, chunk), chunk)],
            send_sem=b_send.at[peer], recv_sem=b_recv.at[me],
            device_id=(peer, core), device_id_type=MESH,
        )

    def arrived_part(peer):
        return pltpu.make_async_remote_copy(
            src_ref=flat.at[pl.ds(pl.multiple_of(peer * chunk, chunk), chunk)],
            dst_ref=parts.at[peer],
            send_sem=a_send.at[peer], recv_sem=a_recv.at[peer],
            device_id=(peer, core), device_id_type=MESH,
        )

    def arrived_whole(peer):
        return pltpu.make_async_remote_copy(
            src_ref=mine,
            dst_ref=whole.at[pl.ds(pl.multiple_of(peer * chunk, chunk), chunk)],
            send_sem=b_send.at[peer], recv_sem=b_recv.at[peer],
            device_id=(peer, core), device_id_type=MESH,
        )

    def loop(body):
        def run(i, carry):
            body(i)
            return carry

        lax.fori_loop(1, n, run, 0)

    loop(lambda i: spread(i).start())
    mine[...] = flat[pl.ds(pl.multiple_of(me * chunk, chunk), chunk), :]

    stage(nbits - 1)
    for g in range(groups):
        proj_out[:, g * gcols:(g + 1) * gcols] = acc[g, 0]

    def add_part(i):
        peer = lax.rem(me + i, n)
        arrived_part(peer).wait_recv()
        mine[...] = mine[...] + parts[peer]

    loop(add_part)
    loop(lambda i: collect(i).start())
    whole[pl.ds(pl.multiple_of(me * chunk, chunk), chunk), :] = mine[...]
    loop(lambda i: arrived_whole(lax.rem(me + i, n)).wait_recv())
    for c in range(cblocks):
        small_out[:, c * LANES:(c + 1) * LANES] = whole[c * per:(c + 1) * per, :]

    loop(lambda i: arrived_part(lax.rem(me + i, n)).wait_send())
    loop(lambda i: arrived_whole(lax.rem(me + i, n)).wait_send())
    for g in range(groups):
        for k in range(nbits):
            stage_copy(g, k).wait_send()

    @pl.when(me > 0)
    def _():
        halo_copy.wait_send()

    for copy in stores:
        copy.wait()


def local(conv_value, conv_gate, conv_out, conv_taps, norm_gain, norm_shift, proj_weight, out_grad):
    rows, chan = conv_value.shape
    ntaps = conv_taps.shape[0]
    width = out_grad.shape[1]
    n = lax.axis_size("sp")
    nbits = n.bit_length() - 1
    assert 1 << nbits == n and lax.axis_size("tp") == 2
    groups = 3
    gcols = chan // groups
    block = width // n
    cblocks = chan // LANES
    halo = 32
    per = -(-(ntaps + 2) // 8) * 8
    chunk = -(-(-(-per * cblocks // n)) // 8) * 8
    dims = (n, nbits, groups, chan * 2)
    taps = conv_taps.astype(F32).reshape(ntaps, cblocks, LANES).transpose(1, 0, 2)
    hbm = pl.BlockSpec(memory_space=pl.ANY)
    vmem = pl.BlockSpec(memory_space=pltpu.VMEM)
    dma = pltpu.SemaphoreType.DMA
    grad_value, grad_gate, small, grad_proj = pl.pallas_call(
        functools.partial(kernel, dims),
        out_shape=(
            jax.ShapeDtypeStruct((rows, chan), BF16),
            jax.ShapeDtypeStruct((rows, chan), BF16),
            jax.ShapeDtypeStruct((per, chan), F32),
            jax.ShapeDtypeStruct((block, chan), F32),
        ),
        in_specs=[hbm, hbm, hbm, vmem, vmem, vmem, hbm, hbm],
        out_specs=(hbm, hbm, vmem, vmem),
        scratch_shapes=[
            pltpu.VMEM((rows, chan), BF16),
            pltpu.VMEM((rows, chan), BF16),
            pltpu.VMEM((rows, chan), BF16),
            pltpu.VMEM((width, chan), BF16),
            pltpu.VMEM((rows, width), BF16),
            pltpu.VMEM((groups, n, block, rows), BF16),
            pltpu.VMEM((rows, chan), BF16),
            pltpu.VMEM((rows, chan), F32),
            pltpu.VMEM((rows, chan), F32),
            pltpu.VMEM((rows, chan), F32),
            pltpu.VMEM((cblocks, rows + halo, LANES), F32),
            pltpu.VMEM((rows, chan), BF16),
            pltpu.VMEM((rows, chan), BF16),
            pltpu.VMEM((rows, LANES), F32),
            pltpu.VMEM((rows, LANES), F32),
            pltpu.VMEM((rows, LANES), F32),
            pltpu.VMEM((rows, LANES), F32),
            pltpu.VMEM((groups, n // 2, block, gcols), F32),
            pltpu.VMEM((groups, n, block, gcols), BF16),
            pltpu.VMEM((groups, n, block, gcols), BF16),
            pltpu.VMEM((cblocks, ntaps, 8, LANES), F32),
            pltpu.VMEM((2, 8, chan), F32),
            pltpu.VMEM((n * chunk, LANES), F32),
            pltpu.VMEM((n, chunk, LANES), F32),
            pltpu.VMEM((chunk, LANES), F32),
            pltpu.VMEM((n * chunk, LANES), F32),
            dma((5,)), dma((2,)),
            dma((2,)), dma((2,)),
            dma, dma,
            dma((groups, nbits)), dma((groups, nbits)),
            dma((n,)), dma((n,)),
            dma((n,)), dma((n,)),
        ],
        compiler_params=pltpu.CompilerParams(
            collective_id=0, has_side_effects=True, vmem_limit_bytes=60 * 1024 * 1024
        ),
    )(
        conv_value, conv_gate, conv_out, taps,
        norm_gain.reshape(1, chan), norm_shift.reshape(1, chan), proj_weight, out_grad,
    )
    return (grad_value, grad_gate, small[:ntaps], small[ntaps], small[ntaps + 1], grad_proj)


def solution(mesh):
    in_specs = (
        P("sp", "tp"),
        P("sp", "tp"),
        P("sp", "tp"),
        P(None, "tp"),
        P("tp"),
        P("tp"),
        P(None, "tp"),
        P("sp", None),
    )
    out_specs = (P("sp", "tp"), P("sp", "tp"), P(None, "tp"), P("tp"), P("tp"), P("sp", "tp"))
    return jax.shard_map(local, mesh=mesh, in_specs=in_specs, out_specs=out_specs, check_vma=False)
```

time: 291 us -> 70.3 us (0.24)
  waiting for transfers between devices: 140 us -> 0 us
  other arithmetic: 57.5 us -> 0 us
  Pallas kernels: 0 us -> 57.3 us
  blocking collectives: 49.3 us -> 0 us
  between operations: 14.5 us -> 0.65 us
  matrix products: 10.2 us -> 0 us
  starting transfers between devices: 6.26 us -> 0 us
    psum x1 -> x0, waiting for transfers between devices: 108 us -> none  [local(): lax.psum((tap_rows, gain_row, shift_row), 'sp')]
    pallas_call x0 -> x1, Pallas kernels: none -> 57.3 us  [local(): pl.pallas_call(functools.partial(kernel, dims), out_shape=(jax.ShapeDtype...]
    psum x4 -> x0, blocking collectives: 49.3 us -> none  [the longest x1 41.7 us: local(): lax.psum((tap_rows, gain_row, shift_row), 'sp')]
    convert_element_type x5 -> x0, other arithmetic: 36.5 us -> none  [the longest x1 30.6 us: local(): (gated_grad * value_float * sig_gate * (1.0 - sig_gate)).astype(jnp.bfloa...]
    reduce_scatter x1 -> x0, waiting for transfers between devices: 32 us -> none  [project_rows(): lax.psum_scatter(lax.dot_general(out_grad, active, (((0,), (0,)), ((), ()...]
    reduce_sum x6 -> x0, other arithmetic: 21 us -> none  [the longest x4 18.1 us: local(): jnp.sum(height_grad * extended[tap_index:tap_index + seq_rows], axis=0)]
    dot_general x2 -> x0, matrix products: 10.2 us -> none  [the longest x1 6.56 us: project_rows(): lax.dot_general(out_grad, active, (((0,), (0,)), ((), ())), preferred_ele...]
    another operation x32 -> x0, local copies, waits for them, and re-layouts: 8.2 us -> none  [local(): jnp.stack([jnp.sum(height_grad * extended[tap_index:tap_index + seq_rows]...]
  transfers between devices with their start and end apart: 4 -> 0, of which waited for: 2 -> 0; matrix products, arithmetic and copies ran while one was open for 24% -> 0% of each run, Pallas kernels for 0% -> 0%
where the time goes in v1:
time: 70.3 us; the launch traced here: 69.9 us
  Pallas kernels  57.3 us (82%)
  local copies, waits for them, and re-layouts  11.9 us (17%)
    pallas_call x1, Pallas kernels, local(): pl.pallas_call(functools.partial(kernel, dims), out_shape=(jax.ShapeDtype...  57.3 us
    unnamed x5, local copies, waits for them, and re-layouts  4.87 us
    slice x1, local copies, waits for them, and re-layouts, local(): small[:ntaps]  1.54 us
    transpose x2, local copies, waits for them, and re-layouts, local(): conv_taps.astype(F32).reshape(ntaps, cblocks, LANES).transpose(1, 0, 2)  1.53 us
    slice x1, local copies, waits for them, and re-layouts, local(): small[ntaps + 1]  1.42 us

profile of v1, /device:TPU:0, one launch (start us, length us, event | category | flops | bytes accessed | tf_op | source)
XLA Modules:
  0.0 69.9 jit_solution(8753278000922141231)
XLA Ops:
  0.6 0.9 %reshape.25 = f32[31,6,128]{2,1,0:T(8,128)S(1)} reshape(bf16[31,768]{1,0:T(8,128)(2,1)} %param.11) | data formatting | bytes 142848 | tf_op jit(solution)/shard_map/transpose | solution.py:412
  1.5 0.7 copy.16
  2.2 1.3 %reshape.23.gain_ref = f32[1,768]{1,0:T(1,128)} reshape(f32[768]{0:T(1024)} %param.12) | data formatting | bytes 6144 | tf_op jit(solution)/shard_map/reshape | solution.py:465
  3.4 1.3 %reshape.24.shift_ref = f32[1,768]{1,0:T(1,128)} reshape(f32[768]{0:T(1024)} %param.13) | data formatting | bytes 6144 | tf_op jit(solution)/shard_map/reshape | solution.py:465
  4.7 57.3 %shard_map.127 = (bf16[512,768]{1,0:T(8,128)(2,1)}, bf16[512,768]{1,0:T(8,128)(2,1)}, f32[40,768]{1,0:T(8,128)}, f32[128,768]{1,0:T(8,128)}) custom-call(bf16[512,768]{1,0:T(8,128)(2,1)} %cv_hbm.1, bf16[512,768]{1,0:T(8,128)(2,1)} %cg_hbm.1, bf16[512,768]{1,0:T(8,128)(2,1)} %co_hbm.1, f32[6,31,128]{2,1,0:T(8,128)} %bitcast.3, f32[1,768]{1,0:T(1,128)} %reshape.23.gain_ref, ...), custom_call_target="tpu_custom_call" | custom-call | tf_op jit(solution)/shard_map/pallas_call | solution.py:416
  62.0 0.0 copy-start
  62.1 1.4 %slice_reduce_fusion = (f32[768]{0:T(1024)}, f32[768]{0:T(1024)}) fusion(f32[40,768]{1,0:T(8,128)} %get-tuple-element.12), kind=kLoop, calls=%fused_computation.1 | loop fusion | bytes 12288 | tf_op jit(solution)/shard_map/slice | solution.py:467
  63.5 1.5 %slice.9 = f32[31,768]{1,0:T(8,128)} slice(f32[40,768]{1,0:T(8,128)} %get-tuple-element.12), slice={[0:31], [0:768]} | slice | bytes 190464 | tf_op jit(solution)/shard_map/slice | solution.py:467
  65.0 2.1 %copy.20 = bf16[512,768]{1,0:T(8,128)(2,1)} copy(bf16[512,768]{1,0:T(8,128)(2,1)} %get-tuple-element.22) | data formatting | bytes 1572864
  67.1 2.1 %copy.21 = bf16[512,768]{1,0:T(8,128)(2,1)} copy(bf16[512,768]{1,0:T(8,128)(2,1)} %get-tuple-element.23) | data formatting | bytes 1572864
  69.1 0.0 copy-done
  69.1 0.7 %copy.22 = f32[128,768]{1,0:T(8,128)} copy(f32[128,768]{1,0:T(8,128)S(1)} %copy-done) | data formatting | bytes 786432
Async XLA Ops:
  62.0 7.1 %copy-start = (f32[128,768]{1,0:T(8,128)S(1)}, f32[128,768]{1,0:T(8,128)}, u32[]{:S(2)}) copy-start(f32[128,768]{1,0:T(8,128)} %get-tuple-element.27) | copy-start | bytes 1179652

commit v2 on v1

--- a/solution.py
+++ b/solution.py
@@ -14,6 +14,17 @@
 LANES = 128
 
 
+def repeat(start, stop, body, unroll):
+    assert (stop - start) % unroll == 0
+
+    def step(i, carry):
+        for u in range(unroll):
+            body(start + i * unroll + u, carry)
+        return carry
+
+    lax.fori_loop(0, (stop - start) // unroll, step, 0)
+
+
 def bit(x, b):
     return lax.rem(x // (1 << b), 2)
 
@@ -46,7 +57,7 @@
     cv_hbm, cg_hbm, co_hbm, taps_ref, gain_ref, shift_ref, w_hbm, og_hbm,
     gv_hbm, gg_hbm, small_out, proj_out,
     cv, cg, co, w, og, ogt, active, normed, dsilu, scaled, hgx, gv, gg,
-    st_a, st_b, st_c, st_d, acc, sendbuf, recvbuf, tapacc, rowacc, flat, parts, mine, whole,
+    st_a, st_b, st_d, pk_a, pk_b, pk_c, pk_d, tapf, acc, sendbuf, recvbuf, tapacc, rowacc, flat, parts, mine, whole,
     in_sem, out_sem, tp_send, tp_recv, halo_send, halo_recv,
     rs_send, rs_recv, a_send, a_recv, b_send, b_recv,
 ):
@@ -56,7 +67,7 @@
     block = width // n
     gcols = chan // groups
     cblocks = chan // LANES
-    ntaps = taps_ref.shape[1]
+    ntaps = taps_ref.shape[0]
     reach = ntaps - 1
     halo = hgx.shape[1] - rows
     chunk = mine.shape[0]
@@ -72,8 +83,7 @@
             ((co_hbm, co), (og_hbm, og), (w_hbm, w), (cg_hbm, cg), (cv_hbm, cv))
         )
     ]
-    for copy in loads:
-        copy.start()
+    loads[0].start()
 
     barrier = pltpu.get_barrier_semaphore()
 
@@ -88,7 +98,27 @@
 
     lane_low = lax.broadcasted_iota(jnp.int32, (1, LANES), 1) < LANES // 2
 
+    gain = gain_ref[...].reshape(1, chan)
+    shift = shift_ref[...].reshape(1, chan)
+    nt = rows // LANES
+    mid = LANES // 2
+
+    def pack(dst):
+        for t in range(nt):
+            turned = st_a[t * LANES:(t + 1) * LANES, :].T
+            dst[0, t:t + 1, :] = turned[:1, :]
+            dst[1, t:t + 1, :] = turned[mid:mid + 1, :]
+
+    def unpack(packed, dst):
+        for t in range(nt):
+            dst[t * LANES:(t + 1) * LANES, :] = jnp.broadcast_to(packed[t:t + 1, :], (LANES, LANES)).T
+
+    def wide(x):
+        return jnp.concatenate([x] * cblocks, axis=1)
+
     loads[0].wait()
+    for copy in loads[1:]:
+        copy.start()
 
     def stats(i, carry):
         at = pl.ds(pl.multiple_of(i * 64, 64), 64)
@@ -99,10 +129,11 @@
         st_a[at, :] = jnp.where(lane_low, mean, m2)
         return carry
 
-    lax.fori_loop(0, rows // 64, stats, 0)
+    repeat(0, rows // 64, stats, 2)
+    pack(pk_a)
     pl.semaphore_wait(barrier, n)
     swap_a = pltpu.make_async_remote_copy(
-        src_ref=st_a, dst_ref=st_b, send_sem=tp_send.at[0], recv_sem=tp_recv.at[0],
+        src_ref=pk_a, dst_ref=pk_b, send_sem=tp_send.at[0], recv_sem=tp_recv.at[0],
         device_id=(me, other_core), device_id_type=MESH,
     )
     swap_a.start()
@@ -126,26 +157,22 @@
     lax.fori_loop(0, width // LANES, transpose, 0)
 
     swap_a.wait()
-    half = 0.5 * chan
+    gap = pk_a[0] - pk_b[0]
+    variance = (pk_a[1] + pk_b[1] + gap * gap * (0.5 * chan)) / chan_total
+    unpack(0.5 * (pk_a[0] + pk_b[0]), st_b)
+    unpack(lax.rsqrt(variance + norm_eps), st_d)
 
     def norm(i, carry):
         at = pl.ds(pl.multiple_of(i * 32, 32), 32)
-        own, peer = st_a[at, :], st_b[at, :]
-        mean_a, mean_b = own[:, :1], peer[:, :1]
-        m2 = own[:, LANES // 2:LANES // 2 + 1] + peer[:, LANES // 2:LANES // 2 + 1]
-        gap = mean_a - mean_b
-        center = 0.5 * (mean_a + mean_b)
-        inv = lax.rsqrt((m2 + gap * gap * half) / chan_total + norm_eps)
-        z = (co[at, :].astype(F32) - center) * inv
+        z = (co[at, :].astype(F32) - wide(st_b[at, :])) * wide(st_d[at, :])
         normed[at, :] = z
-        x = z * gain_ref[...] + shift_ref[...]
+        x = z * gain + shift
         sig = jax.nn.sigmoid(x)
         active[at, :] = (x * sig).astype(BF16)
         dsilu[at, :] = sig * (1.0 + x * (1.0 - sig))
-        st_d[at, :] = jnp.broadcast_to(inv, (32, LANES))
-        return carry
-
-    lax.fori_loop(0, rows // 32, norm, 0)
+        return carry
+
+    repeat(0, rows // 32, norm, 2)
 
     def stage_copy(g, k):
         count = n >> (k + 1)
@@ -224,7 +251,6 @@
         ngz = ng * z
         rowacc[0] = rowacc[0] + jnp.sum(ngz.reshape(4, 8, chan), axis=0)
         rowacc[1] = rowacc[1] + jnp.sum(ng.reshape(4, 8, chan), axis=0)
-        gain = gain_ref[...]
         s = ng * gain
         scaled[at, :] = s
         total = jnp.sum(s, axis=1, keepdims=True)
@@ -232,22 +258,26 @@
         st_a[at, :] = jnp.where(lane_low, total, dot)
         return carry
 
-    lax.fori_loop(0, rows // 32, grads, 0)
+    repeat(0, rows // 32, grads, 2)
+    pack(pk_c)
     swap_b = pltpu.make_async_remote_copy(
-        src_ref=st_a, dst_ref=st_c, send_sem=tp_send.at[1], recv_sem=tp_recv.at[1],
+        src_ref=pk_c, dst_ref=pk_d, send_sem=tp_send.at[1], recv_sem=tp_recv.at[1],
         device_id=(me, other_core), device_id_type=MESH,
     )
     swap_b.start()
     tapacc[...] = jnp.zeros_like(tapacc)
+    for c in range(cblocks):
+        tapf[c] = taps_ref[:, c * LANES:(c + 1) * LANES].astype(F32)
     flat[...] = jnp.zeros_like(flat)
     swap_b.wait()
+    unpack((pk_c[0] + pk_d[0]) / chan_total, st_a)
+    unpack((pk_c[1] + pk_d[1]) / chan_total, st_b)
 
     def height(i, carry):
         at = pl.ds(pl.multiple_of(i * 32, 32), 32)
-        sums = (st_a[at, :] + st_c[at, :]) / chan_total
-        inv = st_d[at, :]
-        total, dot = sums[:, :1], sums[:, LANES // 2:LANES // 2 + 1]
-        hg = inv[:, :1] * (scaled[at, :] - total - normed[at, :] * dot)
+        hg = wide(st_d[at, :]) * (
+            scaled[at, :] - wide(st_a[at, :]) - normed[at, :] * wide(st_b[at, :])
+        )
         for c in range(cblocks):
             hgx[c, at, :] = hg[:, c * LANES:(c + 1) * LANES]
         return carry
@@ -264,7 +294,7 @@
     def _():
         halo_copy.start()
 
-    lax.fori_loop(1, rows // 32, height, 0)
+    repeat(1, rows // 32, height, 3)
 
     @pl.when(me == n - 1)
     def _():
@@ -292,18 +322,16 @@
         total = jnp.zeros((step, LANES), F32)
         for j in range(ntaps):
             h = hgx[c, pl.ds(r + reach - j, step), :]
-            total = total + taps_ref[c, pl.ds(j, 1), :] * h
+            total = total + tapf[c, pl.ds(j, 1), :] * h
             tapacc[c, j] = tapacc[c, j] + jnp.sum((gated * h).reshape(step // 8, 8, LANES), axis=0)
         gv[at, cols] = (total * sig).astype(BF16)
         gg[at, cols] = (total * value * sig * (1.0 - sig)).astype(BF16)
         return carry
 
-    cuts = [cblocks * steps * i // nbits for i in range(nbits + 1)]
-    for k in range(nbits - 1):
-        lax.fori_loop(cuts[k], cuts[k + 1], conv, 0)
-        if k + 1 < nbits - 1:
-            stage(k + 1)
-    lax.fori_loop(cuts[nbits - 1], cuts[nbits], conv, 0)
+    cut = cblocks * steps * 3 // 4
+    lax.fori_loop(0, cut, conv, 0)
+    stage(1)
+    lax.fori_loop(cut, cblocks * steps, conv, 0)
 
     stores = [
         pltpu.make_async_copy(src, dst, out_sem.at[i])
@@ -364,9 +392,8 @@
     loop(lambda i: spread(i).start())
     mine[...] = flat[pl.ds(pl.multiple_of(me * chunk, chunk), chunk), :]
 
-    stage(nbits - 1)
-    for g in range(groups):
-        proj_out[:, g * gcols:(g + 1) * gcols] = acc[g, 0]
+    for k in range(2, nbits - 1):
+        stage(k)
 
     def add_part(i):
         peer = lax.rem(me + i, n)
@@ -376,6 +403,10 @@
     loop(add_part)
     loop(lambda i: collect(i).start())
     whole[pl.ds(pl.multiple_of(me * chunk, chunk), chunk), :] = mine[...]
+
+    stage(nbits - 1)
+    for g in range(groups):
+        proj_out[:, g * gcols:(g + 1) * gcols] = acc[g, 0]
     loop(lambda i: arrived_whole(lax.rem(me + i, n)).wait_recv())
     for c in range(cblocks):
         small_out[:, c * LANES:(c + 1) * LANES] = whole[c * per:(c + 1) * per, :]
@@ -391,6 +422,28 @@
         halo_copy.wait_send()
 
     for copy in stores:
+        copy.wait()
+
+
+def place(gv_in, gg_in, small, proj_in, gv_out, gg_out, taps, gain, shift, proj_out, gv, gg, proj, in_sem, out_sem):
+    ins = [
+        pltpu.make_async_copy(src, dst, in_sem.at[i])
+        for i, (src, dst) in enumerate(((gv_in, gv), (gg_in, gg), (proj_in, proj)))
+    ]
+    outs = [
+        pltpu.make_async_copy(src, dst, out_sem.at[i])
+        for i, (src, dst) in enumerate(((gv, gv_out), (gg, gg_out), (proj, proj_out)))
+    ]
+    for copy in ins:
+        copy.start()
+    ntaps = taps.shape[0]
+    taps[...] = small[:ntaps, :]
+    gain[...] = small[ntaps, :]
+    shift[...] = small[ntaps + 1, :]
+    for came, goes in zip(ins, outs):
+        came.wait()
+        goes.start()
+    for copy in outs:
         copy.wait()
 
 
@@ -409,7 +462,6 @@
     per = -(-(ntaps + 2) // 8) * 8
     chunk = -(-(-(-per * cblocks // n)) // 8) * 8
     dims = (n, nbits, groups, chan * 2)
-    taps = conv_taps.astype(F32).reshape(ntaps, cblocks, LANES).transpose(1, 0, 2)
     hbm = pl.BlockSpec(memory_space=pl.ANY)
     vmem = pl.BlockSpec(memory_space=pltpu.VMEM)
     dma = pltpu.SemaphoreType.DMA
@@ -440,7 +492,8 @@
             pltpu.VMEM((rows, LANES), F32),
             pltpu.VMEM((rows, LANES), F32),
             pltpu.VMEM((rows, LANES), F32),
-            pltpu.VMEM((rows, LANES), F32),
+            *[pltpu.VMEM((2, rows // LANES, LANES), F32)] * 4,
+            pltpu.VMEM((cblocks, ntaps, LANES), F32),
             pltpu.VMEM((groups, n // 2, block, gcols), F32),
             pltpu.VMEM((groups, n, block, gcols), BF16),
             pltpu.VMEM((groups, n, block, gcols), BF16),
@@ -461,10 +514,27 @@
             collective_id=0, has_side_effects=True, vmem_limit_bytes=60 * 1024 * 1024
         ),
     )(
-        conv_value, conv_gate, conv_out, taps,
-        norm_gain.reshape(1, chan), norm_shift.reshape(1, chan), proj_weight, out_grad,
+        conv_value, conv_gate, conv_out, conv_taps, norm_gain, norm_shift, proj_weight, out_grad,
     )
-    return (grad_value, grad_gate, small[:ntaps], small[ntaps], small[ntaps + 1], grad_proj)
+    return pl.pallas_call(
+        place,
+        out_shape=(
+            jax.ShapeDtypeStruct((rows, chan), BF16),
+            jax.ShapeDtypeStruct((rows, chan), BF16),
+            jax.ShapeDtypeStruct((ntaps, chan), F32),
+            jax.ShapeDtypeStruct((chan,), F32),
+            jax.ShapeDtypeStruct((chan,), F32),
+            jax.ShapeDtypeStruct((block, chan), F32),
+        ),
+        in_specs=[hbm, hbm, vmem, hbm],
+        out_specs=(hbm, hbm, vmem, vmem, vmem, hbm),
+        scratch_shapes=[
+            pltpu.VMEM((rows, chan), BF16),
+            pltpu.VMEM((rows, chan), BF16),
+            pltpu.VMEM((block, chan), F32),
+            dma((3,)), dma((3,)),
+        ],
+    )(grad_value, grad_gate, small, grad_proj)
 
 
 def solution(mesh):

time: 70.3 us -> 57.3 us (0.82)
  local copies, waits for them, and re-layouts: 11.9 us -> 0 us
  Pallas kernels: 57.3 us -> 56.4 us
    pallas_call x1, Pallas kernels: 57.3 us -> 52.4 us  [local(): pl.pallas_call(functools.partial(kernel, dims), out_shape=(jax.ShapeDtype...]
    unnamed x5 -> x0, local copies, waits for them, and re-layouts: 4.87 us -> none
    pallas_call x0 -> x1, Pallas kernels: none -> 4 us  [local(): pl.pallas_call(place, out_shape=(jax.ShapeDtypeStruct((rows, chan), BF16)...]
    slice x2 -> x0, local copies, waits for them, and re-layouts: 2.96 us -> none  [the longest x1 1.54 us: local(): small[:ntaps]]
    reshape x2 -> x0, local copies, waits for them, and re-layouts: 2.53 us -> none  [the longest x1 1.27 us: local(): norm_shift.reshape(1, chan)]
    transpose x2 -> x0, local copies, waits for them, and re-layouts: 1.53 us -> none  [local(): conv_taps.astype(F32).reshape(ntaps, cblocks, LANES).transpose(1, 0, 2)]
where the time goes in v2:
time: 57.3 us; the launch traced here: 57 us
  Pallas kernels  56.4 us (98%)
  between operations  0.64 us (1%)
    pallas_call x1, Pallas kernels, local(): pl.pallas_call(functools.partial(kernel, dims), out_shape=(jax.ShapeDtype...  52.4 us
    pallas_call x1, Pallas kernels, local(): pl.pallas_call(place, out_shape=(jax.ShapeDtypeStruct((rows, chan), BF16)...  4 us

profile of v2, /device:TPU:0, one launch (start us, length us, event | category | flops | bytes accessed | tf_op | source)
XLA Modules:
  0.0 57.0 jit_solution(2418023187647917226)
XLA Ops:
  0.6 52.4 %shard_map.127 = (bf16[512,768]{1,0:T(8,128)(2,1)}, bf16[512,768]{1,0:T(8,128)(2,1)}, f32[40,768]{1,0:T(8,128)}, f32[128,768]{1,0:T(8,128)}) custom-call(bf16[512,768]{1,0:T(8,128)(2,1)} %cv_hbm.1, bf16[512,768]{1,0:T(8,128)(2,1)} %cg_hbm.1, bf16[512,768]{1,0:T(8,128)(2,1)} %co_hbm.1, bf16[31,768]{1,0:T(8,128)(2,1)} %taps_ref.1, f32[768]{0:T(1024)} %gain_ref.1, ...), custom_call_target="tpu_custom_call" | custom-call | tf_op jit(solution)/shard_map/pallas_call | solution.py:468
  53.0 4.0 %shard_map.128 = (bf16[512,768]{1,0:T(8,128)(2,1)}, bf16[512,768]{1,0:T(8,128)(2,1)}, f32[31,768]{1,0:T(8,128)}, f32[768]{0:T(1024)}, f32[768]{0:T(1024)}, /*index=5*/f32[128,768]{1,0:T(8,128)}) custom-call(bf16[512,768]{1,0:T(8,128)(2,1)} %get-tuple-element.10.gv_in, bf16[512,768]{1,0:T(8,128)(2,1)} %get-tuple-element.11.gg_in, ...), custom_call_target="tpu_custom_call" | custom-call | tf_op jit(solution)/shard_map/pallas_call | solution.py:519

commit v3 on v2

--- a/solution.py
+++ b/solution.py
@@ -201,14 +201,6 @@
 
         lax.fori_loop(0, n // 2 // unit, far, 0)
         stage_copy(g, 0).start()
-    for g in range(groups):
-
-        def near(i, carry, g=g):
-            acc[g, pl.ds(i * unit, unit)] = product(g, i * unit)
-            return carry
-
-        lax.fori_loop(0, n // 2 // unit, near, 0)
-
     def stage(k):
         count = n >> (k + 1)
         off = n - (n >> k)
@@ -269,6 +261,14 @@
     for c in range(cblocks):
         tapf[c] = taps_ref[:, c * LANES:(c + 1) * LANES].astype(F32)
     flat[...] = jnp.zeros_like(flat)
+    for g in range(groups):
+
+        def near(i, carry, g=g):
+            acc[g, pl.ds(i * unit, unit)] = product(g, i * unit)
+            return carry
+
+        lax.fori_loop(0, n // 2 // unit, near, 0)
+
     swap_b.wait()
     unpack((pk_c[0] + pk_d[0]) / chan_total, st_a)
     unpack((pk_c[1] + pk_d[1]) / chan_total, st_b)

time: 57.3 us -> 57.3 us (level)
  no operation moved by 1% of the time
where the time goes in v3:
time: 57.3 us; the launch traced here: 57 us
  Pallas kernels  56.4 us (98%)
  between operations  0.64 us (1%)
    pallas_call x1, Pallas kernels, local(): pl.pallas_call(functools.partial(kernel, dims), out_shape=(jax.ShapeDtype...  52.4 us
    pallas_call x1, Pallas kernels, local(): pl.pallas_call(place, out_shape=(jax.ShapeDtypeStruct((rows, chan), BF16)...  4 us

profile of v3, /device:TPU:0, one launch (start us, length us, event | category | flops | bytes accessed | tf_op | source)
XLA Modules:
  0.0 57.0 jit_solution(16691659044328701093)
XLA Ops:
  0.6 52.4 %shard_map.127 = (bf16[512,768]{1,0:T(8,128)(2,1)}, bf16[512,768]{1,0:T(8,128)(2,1)}, f32[40,768]{1,0:T(8,128)}, f32[128,768]{1,0:T(8,128)}) custom-call(bf16[512,768]{1,0:T(8,128)(2,1)} %cv_hbm.1, bf16[512,768]{1,0:T(8,128)(2,1)} %cg_hbm.1, bf16[512,768]{1,0:T(8,128)(2,1)} %co_hbm.1, bf16[31,768]{1,0:T(8,128)(2,1)} %taps_ref.1, f32[768]{0:T(1024)} %gain_ref.1, ...), custom_call_target="tpu_custom_call" | custom-call | tf_op jit(solution)/shard_map/pallas_call | solution.py:468
  53.0 4.0 %shard_map.128 = (bf16[512,768]{1,0:T(8,128)(2,1)}, bf16[512,768]{1,0:T(8,128)(2,1)}, f32[31,768]{1,0:T(8,128)}, f32[768]{0:T(1024)}, f32[768]{0:T(1024)}, /*index=5*/f32[128,768]{1,0:T(8,128)}) custom-call(bf16[512,768]{1,0:T(8,128)(2,1)} %get-tuple-element.10.gv_in, bf16[512,768]{1,0:T(8,128)(2,1)} %get-tuple-element.11.gg_in, ...), custom_call_target="tpu_custom_call" | custom-call | tf_op jit(solution)/shard_map/pallas_call | solution.py:519
